TPU v7x, 32 devices: a whole 2x2x4 slice. The times are simulated.
32 devices in a mesh: grp: 2 (over y), ep: 8 (over z, x), tp: 2 (over core).
Axes of the slice: x: 2, y: 2, z: 4, core: 2. Of those that a mesh axis runs over, the one named last changes fastest.
Arguments:
- tokens: bfloat16 [8192, 2048], P(('grp', 'ep', 'tp')), parts along dimension 0, may hold values from -15 to 15
- gain_in: float32 [2048], replicated, may hold values from 0.1 to 1.9
- expert_ids: int32 [8192, 2], P(('grp', 'ep')), parts along dimension 0, may hold values from 0 to 7, all different within a row; in each aligned block of 256 rows (0 to 255, 256 to 511, ...) at most 128 rows name the same one
- gate_weights: float32 [8192, 2], P(('grp', 'ep')), parts along dimension 0, may hold values from 0.1 to 1
- w_gate: bfloat16 [8, 2048, 512], P('ep', None, 'tp'), may hold values from -0.125 to 0.125
- w_up: bfloat16 [8, 2048, 512], P('ep', None, 'tp'), may hold values from -0.125 to 0.125
- w_down: bfloat16 [8, 2048, 512], P('ep', None, 'tp'), may hold values from -20 to 20
- gain_out: float32 [2048], P('tp'), may hold values from 0.1 to 1.9
Outputs:
- mixed: bfloat16 [8192, 2048], P(('grp', 'ep'), 'tp'), parts along dimension 0
There are 2 independent parts, one for each index of `grp`. A program takes and returns all parts, laid end to end along the dimension named above; an argument that names none is the same for every part. Nothing has to cross between parts.
Inputs may be any that keep to these rules, and one draw needn't show every extreme that they name: `expert_ids`: each token names 2 different experts; in each aligned block of 256 tokens no expert is named by more than 128 pairs, a bound that some block reaches.
All inputs are finite; a program needn't handle non-finite values.
Results may differ from a plain program's by a relative error of at most 0.0077.
Values may be sent and summed in bfloat16 or wider, within the bound.
A program may use at most 64 MiB of HBM per device.

v0:
```python
import functools

import jax
import jax.numpy as jnp
from jax import lax
from jax.experimental import pallas as pl
from jax.experimental.pallas import tpu as pltpu
from jax.sharding import PartitionSpec as P

EPS = 1e-06
MESH = pl.DeviceIdType.MESH
NT = (((1,), (1,)), ((), ()))
TN = (((0,), (0,)), ((), ()))


def plane_width(ep):
    return max(n for n in range(1, ep + 1) if ep % n == 0 and n**3 <= ep)


def kernel(
    G, X, Z, F, cap,
    tokens_ref, gain_in_ref, meta_ref, wg_ref, wu_ref, wd_ref, gain_out_ref,
    out_ref,
    wbuf, tok, meta, acc, comb, rows, hid, pick, gslot, gains, inbox,
    wsem, wx_send, wy_send, wt_send, tok_recv, tok_send, meta_recv, meta_send,
    acc_recv, acc_send, misc_recv, misc_send, load_sem,
):
    g, ep, c = lax.axis_index("grp"), lax.axis_index("ep"), lax.axis_index("tp")
    z, x = ep // X, lax.rem(ep, X)
    other = 1 - c
    T = tokens_ref.shape[0]
    D = tokens_ref.shape[1]
    C = D // F
    H = wg_ref.shape[-1]
    FG = F // G
    weights = (wg_ref, wu_ref, wd_ref)

    def arrived(ref, sem):
        pltpu.make_async_copy(ref, ref, sem).wait()

    def send(src, dst, ssem, rsem, **where):
        return pltpu.make_async_remote_copy(
            src_ref=src, dst_ref=dst, send_sem=ssem, recv_sem=rsem,
            device_id=where, device_id_type=MESH,
        )

    def wslice(p, half, kind, q):
        return wbuf.at[p, half, kind, q]

    def load(f):
        return pltpu.make_async_copy(tokens_ref.at[:, f * C : (f + 1) * C], tok.at[z, f], load_sem.at[f])

    for f in range(F):
        load(f).start()

    for kind in range(3):
        for q in range(F):
            pltpu.make_async_copy(
                weights[kind].at[q], wslice(x, c, kind, q), wsem.at[x, c, kind, q]
            ).start()

    barrier = pltpu.get_barrier_semaphore()
    for i in range(1, Z):
        pl.semaphore_signal(barrier, inc=1, device_id={"ep": lax.rem(z + i, Z) * X + x}, device_id_type=MESH)
    for i in range(1, X):
        pl.semaphore_signal(barrier, inc=1, device_id={"ep": z * X + lax.rem(x + i, X)}, device_id_type=MESH)
    for i in range(1, G):
        pl.semaphore_signal(barrier, inc=1, device_id={"grp": lax.rem(g + i, G)}, device_id_type=MESH)
    pl.semaphore_signal(barrier, inc=1, device_id={"tp": other}, device_id_type=MESH)

    square = jnp.zeros((T, 1), jnp.float32)
    for f in range(F):
        load(f).wait()
        value = tok[z, f].astype(jnp.float32)
        square = square + jnp.sum(value * value, axis=1, keepdims=True)
    inv = lax.rsqrt(square / D + EPS)
    for f in range(F):
        gain = gain_in_ref[:, f * C : (f + 1) * C]
        tok[z, f] = (tok[z, f].astype(jnp.float32) * inv * gain).astype(jnp.bfloat16)

    pl.semaphore_wait(barrier, Z + X + G - 2)

    def to_line(i):
        return send(
            meta_ref, meta.at[z], meta_send.at[i], meta_recv.at[z], ep=lax.rem(z + i, Z) * X + x
        )

    for i in range(1, Z):
        to_line(i).start()

    def along(b, f, way):
        step = 1 if way == 0 else -1
        return send(
            tok.at[b, f], tok.at[b, f], tok_send.at[way, b, f], tok_recv.at[b, f], ep=(z + step) * X + x
        )

    can = (z < Z - 1, z > 0)
    for f in range(F):
        for way in range(2):
            pl.when(can[way])(lambda f=f, way=way: along(z, f, way).start())

    def to_plane(i, kind, j):
        q = g * FG + j
        return send(
            weights[kind].at[q], wslice(x, c, kind, q), wx_send.at[i, kind, j],
            wsem.at[x, c, kind, q], ep=z * X + lax.rem(x + i, X),
        )

    for kind in range(3):
        for j in range(FG):
            for i in range(1, X):
                to_plane(i, kind, j).start()

    gain_copy = send(gain_out_ref, gains.at[1], misc_send.at[0], misc_recv.at[0], tp=other)
    gain_copy.start()
    gains[0] = gain_out_ref[...]
    meta[z] = meta_ref[...]

    def to_core(p, kind, q):
        return send(
            wslice(p, c, kind, q), wslice(p, c, kind, q), wt_send.at[p, kind, q],
            wsem.at[p, c, kind, q], tp=other,
        )

    def to_group(p, i, kind, j):
        q = g * FG + j
        return send(
            wslice(p, c, kind, q), wslice(p, c, kind, q), wy_send.at[p, i, kind, j],
            wsem.at[p, c, kind, q], grp=lax.rem(g + i, G),
        )

    for kind in range(3):
        for q in range(F):
            arrived(wslice(x, c, kind, q), wsem.at[x, c, kind, q])
            to_core(x, kind, q).start()

    def from_plane(n):
        kind, j = n // FG, n % FG
        q = g * FG + j
        for i in range(1, X):
            p = lax.rem(x + i, X)
            arrived(wslice(p, c, kind, q), wsem.at[p, c, kind, q])
            for i2 in range(1, G):
                to_group(p, i2, kind, j).start()
            to_core(p, kind, q).start()

    def from_group(n):
        kind, j = n // FG, n % FG
        for i in range(1, X):
            p = lax.rem(x + i, X)
            for i2 in range(1, G):
                q = lax.rem(g + i2, G) * FG + j
                arrived(wslice(p, c, kind, q), wsem.at[p, c, kind, q])
                to_core(p, kind, q).start()

    def from_core(kind):
        for p in range(X):
            for q in range(F):
                arrived(wslice(p, other, kind, q), wsem.at[p, other, kind, q])

    def relay(d, f):
        for way in range(2):
            b = z - d if way == 0 else z + d
            have = b >= 0 if way == 0 else b < Z

            @pl.when(have)
            def _():
                arrived(tok.at[b, f], tok_recv.at[b, f])
                pl.when(can[way])(lambda: along(b, f, way).start())

    def hidden(b):
        m = meta[b]
        expert = (lax.broadcasted_iota(jnp.int32, (8, T), 0) + z * X).astype(jnp.float32)
        first, second = m[0:1] == expert, m[1:2] == expert
        named = jnp.where(first | second, 1.0, 0.0)
        gate = jnp.where(first, m[2:3], 0.0) + jnp.where(second, m[3:4], 0.0)
        line = lax.broadcasted_iota(jnp.int32, (T, T), 0)
        earlier = jnp.where(line < lax.broadcasted_iota(jnp.int32, (T, T), 1), 1.0, 0.0)
        before = jnp.dot(
            named.astype(jnp.bfloat16), earlier.astype(jnp.bfloat16), preferred_element_type=jnp.float32
        )
        place = jnp.where(named > 0.0, before, -1.0)
        slot = lax.broadcasted_iota(jnp.int32, (cap, T), 0).astype(jnp.float32)
        for p in range(X):
            hit = place[p : p + 1] == slot
            pick[b, p * cap : (p + 1) * cap] = jnp.where(hit, 1.0, 0.0).astype(jnp.bfloat16)
            weight = jnp.sum(jnp.where(hit, gate[p : p + 1], 0.0), axis=1, keepdims=True)
            gslot[b, p * cap : (p + 1) * cap] = jnp.broadcast_to(weight, (cap, 128))
        for f in range(F):
            rows[:, f * C : (f + 1) * C] = jnp.dot(
                pick[b], tok[b, f], preferred_element_type=jnp.float32
            ).astype(jnp.bfloat16)
        for p in range(X):
            here = rows[p * cap : (p + 1) * cap]
            for half in range(2):
                gated = jnp.dot(here, wbuf[p, half, 0].reshape(D, H), preferred_element_type=jnp.float32)
                up = jnp.dot(here, wbuf[p, half, 1].reshape(D, H), preferred_element_type=jnp.float32)
                value = gated / (1.0 + jnp.exp(-gated)) * up
                hid[b, p * cap : (p + 1) * cap, half * H : (half + 1) * H] = value.astype(jnp.bfloat16)

    def partial(b, f):
        parts = []
        for p in range(X):
            span = slice(p * cap, (p + 1) * cap)
            y = lax.dot_general(
                hid[b, span, 0:H], wbuf[p, 0, 2, f], NT, preferred_element_type=jnp.float32
            ) + lax.dot_general(
                hid[b, span, H : 2 * H], wbuf[p, 1, 2, f], NT, preferred_element_type=jnp.float32
            )
            parts.append((y * gslot[b, span, 0:1]).astype(jnp.bfloat16))
        return lax.dot_general(
            pick[b], jnp.concatenate(parts, axis=0), TN, preferred_element_type=jnp.float32
        )

    def both_hidden(d):
        def side(s, carry):
            b = z + d * (2 * s - 1)
            pl.when((b >= 0) & (b < Z))(lambda: hidden(b))
            return carry

        lax.fori_loop(0, 2, side, 0)

    def onward(b, f, way):
        step = 1 - 2 * way
        to = jnp.where((way == 1) & (z - 1 == b), Z, b)
        return send(
            acc.at[b, f], acc.at[to, f], acc_send.at[b, f], acc_recv.at[to, f], ep=(z + step) * X + x
        )

    def sums(d, low, high):
        def chunk(i, carry):
            f = i // 2
            turn = lax.rem(i, 2)
            way = jnp.where(2 * z < Z, turn, 1 - turn)
            b = jnp.where(way == 0, d, Z - 1 - d)
            active = jnp.where(way == 0, b - z, z - b) > 0
            fed = jnp.where(way == 0, z, Z - 1 - z) > 0

            @pl.when(active & fed)
            def _():
                part = partial(b, f)
                arrived(acc.at[b, f], acc_recv.at[b, f])
                acc[b, f] = (part + acc[b, f].astype(jnp.float32)).astype(jnp.bfloat16)
                onward(b, f, way).start()

            @pl.when(active & jnp.logical_not(fed))
            def _():
                acc[b, f] = partial(b, f).astype(jnp.bfloat16)
                onward(b, f, way).start()

            return carry

        lax.fori_loop(2 * low, 2 * high, chunk, 0)

    pieces = 3 * FG
    for n in range(max(pieces, F)):
        if n < F:
            relay(1, n)
        elif Z > 2 and n - F < F:
            relay(2, n - F)
        if n < pieces:
            from_plane(n)
        if 1 <= n <= pieces:
            from_group(n - 1)
    if pieces >= F:
        from_group(pieces - 1)
    done = max(pieces, F) - F
    for i in range(1, Z):
        b = lax.rem(z + i, Z)
        arrived(meta.at[b], meta_recv.at[b])
    from_core(0)
    from_core(1)
    both_hidden(1)
    from_core(2)
    early = F // 4
    sums(1, 0, early)
    if Z > 2:
        for f in range(done, F):
            relay(2, f)
        both_hidden(2)

    if Z > 2:
        sums(2, 0, F)

    def stage(d, carry):
        def one(f, inner):
            relay(d, f)
            return inner

        lax.fori_loop(0, F, one, 0)
        both_hidden(d)
        sums(d, 0, F)
        return carry

    lax.fori_loop(3, Z, stage, 0)
    sums(1, early, F)

    hidden(z)
    total = jnp.zeros((T, 1), jnp.float32)
    for f in range(F):
        comb[f] = partial(z, f)
    for f in range(F):

        @pl.when(z > 0)
        def _():
            arrived(acc.at[z, f], acc_recv.at[z, f])
            comb[f] = comb[f] + acc[z, f].astype(jnp.float32)

        @pl.when(z < Z - 1)
        def _():
            arrived(acc.at[Z, f], acc_recv.at[Z, f])
            comb[f] = comb[f] + acc[Z, f].astype(jnp.float32)

        value = comb[f]
        total = total + jnp.sum(value * value, axis=1, keepdims=True)
    scale = lax.rsqrt(total / D + EPS)
    arrived(gains.at[1], misc_recv.at[0])
    half = F // 2
    for f in range(F):
        pl.when(can[0])(lambda f=f: along(z, f, 0).wait_send())
        pl.when(can[1])(lambda f=f: along(z, f, 1).wait_send())
    for f in range(half):
        gain = gains[1, :, f * C : (f + 1) * C]
        tok[z, f] = (comb[other * half + f] * scale * gain).astype(jnp.bfloat16)
    out_copy = send(tok.at[z, :half], inbox, misc_send.at[1], misc_recv.at[1], tp=other)
    out_copy.start()
    for f in range(half):
        gain = gains[0, :, f * C : (f + 1) * C]
        out_ref[c, :, f * C : (f + 1) * C] = (comb[c * half + f] * scale * gain).astype(jnp.bfloat16)

    gain_copy.wait_send()
    for i in range(1, Z):
        to_line(i).wait_send()
    for kind in range(3):
        for i in range(1, X):
            p = lax.rem(x + i, X)
            for j in range(FG):
                to_plane(i, kind, j).wait_send()
                for i2 in range(1, G):
                    to_group(p, i2, kind, j).wait_send()
        for p in range(X):
            for q in range(F):
                to_core(p, kind, q).wait_send()

    def drain(b, carry):
        for f in range(F):
            pl.when(can[0] & (b < z))(lambda f=f: along(b, f, 0).wait_send())
            pl.when(can[1] & (b > z))(lambda f=f: along(b, f, 1).wait_send())
            pl.when(b != z)(lambda f=f: onward(b, f, 0).wait_send())
        return carry

    lax.fori_loop(0, Z, drain, 0)
    out_copy.wait()
    for f in range(half):
        out_ref[other, :, f * C : (f + 1) * C] = inbox[f]


def per_device(G, X, Z, tokens, gain_in, expert_ids, gate_weights, w_gate, w_up, w_down, gain_out):
    T, D = tokens.shape
    top = expert_ids.shape[1]
    cap = 2 * T * top // (X * Z)
    H = w_gate.shape[2]
    F = 4
    C = D // F
    first = lax.axis_index("tp") * T
    ids = lax.dynamic_slice_in_dim(expert_ids, first, T, 0).astype(jnp.float32)
    gates = lax.dynamic_slice_in_dim(gate_weights, first, T, 0)
    meta = jnp.concatenate([ids.T, gates.T, jnp.zeros((8 - 2 * top, T), jnp.float32)], axis=0)
    vmem = pl.BlockSpec(memory_space=pltpu.VMEM)
    hbm = pl.BlockSpec(memory_space=pl.ANY)
    bf16, f32 = jnp.bfloat16, jnp.float32
    dma = pltpu.SemaphoreType.DMA
    R = X * cap
    out = pl.pallas_call(
        functools.partial(kernel, G, X, Z, F, cap),
        out_shape=jax.ShapeDtypeStruct((2, T, D // 2), bf16),
        in_specs=[hbm, vmem, vmem, hbm, hbm, hbm, vmem],
        out_specs=vmem,
        scratch_shapes=[
            pltpu.VMEM((X, 2, 3, F, C, H), bf16),
            pltpu.VMEM((Z, F, T, C), bf16),
            pltpu.VMEM((Z, 8, T), f32),
            pltpu.VMEM((Z + 1, F, T, C), bf16),
            pltpu.VMEM((F, T, C), f32),
            pltpu.VMEM((R, D), bf16),
            pltpu.VMEM((Z, R, 2 * H), bf16),
            pltpu.VMEM((Z, R, T), bf16),
            pltpu.VMEM((Z, R, 128), f32),
            pltpu.VMEM((2, 1, D // 2), f32),
            pltpu.VMEM((F // 2, T, C), bf16),
            dma((X, 2, 3, F)),
            dma((X, 3, F // G)),
            dma((X, G, 3, F // G)),
            dma((X, 3, F)),
            dma((Z, F)),
            dma((2, Z, F)),
            dma((Z,)),
            dma((Z,)),
            dma((Z + 1, F)),
            dma((Z, F)),
            dma((2,)),
            dma((2,)),
            dma((F,)),
        ],
        compiler_params=pltpu.CompilerParams(
            collective_id=0, has_side_effects=True, vmem_limit_bytes=67043328
        ),
    )(
        tokens, gain_in.reshape(1, D), meta,
        w_gate.reshape(F, C, H), w_up.reshape(F, C, H), w_down.reshape(F, C, H),
        gain_out.reshape(1, D // 2),
    )
    return out.reshape(2 * T, D // 2)


def solution(mesh):
    placed = (
        P(("grp", "ep", "tp"), None),
        P(),
        P(("grp", "ep"), None),
        P(("grp", "ep"), None),
        P("ep", None, "tp"),
        P("ep", None, "tp"),
        P("ep", None, "tp"),
        P("tp"),
    )
    X = plane_width(mesh.shape["ep"])
    body = functools.partial(per_device, mesh.shape["grp"], X, mesh.shape["ep"] // X)
    return jax.shard_map(
        body, mesh=mesh, in_specs=placed, out_specs=P(("grp", "ep"), "tp"), check_vma=False
    )
```

profile of v0, /device:TPU:11, one launch (start us, length us, event | category | flops | bytes accessed | tf_op | source)
XLA Modules:
  0.0 126.5 jit_solution(18023081745089715732)
XLA Ops:
  0.0 0.0 copy-start
  0.0 0.0 copy-start.1
  0.0 0.1 pad.2.clone
  0.1 0.6 copy-done
  0.7 0.0 copy-done.1
  0.7 0.7 maximum_maximum_fusion.meta_ref
  1.4 122.9 %shard_map.82 = bf16[2,256,1024]{2,1,0:T(8,128)(2,1)} custom-call(bf16[256,2048]{1,0:T(8,128)(2,1)} %tokens_ref.1, f32[1,2048]{1,0:T(1,128)} %bitcast.14, f32[8,256]{1,0:T(8,128)} %maximum_maximum_fusion.meta_ref, bf16[4,512,256]{2,1,0:T(8,128)(2,1)} %bitcast.11, bf16[4,512,256]{2,1,0:T(8,128)(2,1)} %bitcast.12, bf16[4,512,256]{2,1,0:T(8,128)(2,1)} %bitcast.13, ...), custom_call_target="tpu_custom_call" | custom-call | tf_op jit(solution)/shard_map/pallas_call | solution.py:374
  124.2 2.3 %copy.10 = bf16[512,1024]{1,0:T(8,128)(2,1)} copy(bf16[512,1024]{1,0:T(8,128)(2,1)} %bitcast.10) | data formatting | bytes 2097152
  (3 shorter events, 0.0 us)
Async XLA Ops:
  0.0 0.7 copy-start
  0.0 0.7 copy-start.1
where the time goes:
time: 128 us; the launch traced here: 126 us
  Pallas kernels  123 us (96%)
  local copies, waits for them, and re-layouts  2.96 us (2%)
    pallas_call x1, Pallas kernels, per_device(): pl.pallas_call(functools.partial(kernel, G, X, Z, F, cap), out_shape=jax....  123 us
    unnamed x5, local copies, waits for them, and re-layouts  2.88 us

commit v1 on v0

--- a/solution.py
+++ b/solution.py
@@ -355,28 +355,484 @@
         out_ref[other, :, f * C : (f + 1) * C] = inbox[f]
 
 
+def quad_kernel(
+    G, X, Z, F, cap,
+    tokens_ref, gain_in_ref, ids_ref, gates_ref, wg_ref, wu_ref, wd_ref, gain_out_ref,
+    out_ref,
+    wbuf, tok, meta, acc, comb, rows, gated, hid, pick, gslot, gains, stage, ids, gates,
+    own_sem, nat_sem, plane_sem, group_sem, wide_sem, down_sem, wx_send, wy_send, wt_send,
+    tok_recv, tok_send, meta_recv, meta_send, acc_recv, acc_send,
+    gain_recv, gain_send, out_recv, out_send, load_sem, pair_sem,
+):
+    g, ep, c = lax.axis_index("grp"), lax.axis_index("ep"), lax.axis_index("tp")
+    z, x = ep // X, lax.rem(ep, X)
+    other = 1 - c
+    T, D = tokens_ref.shape
+    C = D // F
+    W, C2, H = wg_ref.shape
+    R = X * cap
+    FG, WG = F // G, W // G
+    SUB = W // F
+    LEAD = F // 2
+    LAG = 3
+    weights = (wg_ref, wu_ref, wd_ref)
+    is_end = (z == 0) | (z == Z - 1)
+    is_inner = jnp.logical_not(is_end)
+    s = jnp.where(2 * z < Z, 1, -1)
+    IN, OUT = 0, 1
+
+    def arrived(ref, sem):
+        pltpu.make_async_copy(ref, ref, sem).wait()
+
+    def send(src, dst, ssem, rsem, **where):
+        return pltpu.make_async_remote_copy(
+            src_ref=src, dst_ref=dst, send_sem=ssem, recv_sem=rsem,
+            device_id=where, device_id_type=MESH,
+        )
+
+    def load(f):
+        return pltpu.make_async_copy(tokens_ref.at[:, f * C : (f + 1) * C], tok.at[z, f], load_sem)
+
+    def load_own(kind):
+        return pltpu.make_async_copy(weights[kind], wbuf.at[x, c, kind], own_sem.at[kind])
+
+    mine = pl.ds(pl.multiple_of(c * T, T), T)
+    load_ids = pltpu.make_async_copy(ids_ref.at[:, mine], ids, pair_sem.at[0])
+    load_gates = pltpu.make_async_copy(gates_ref.at[:, mine], gates, pair_sem.at[1])
+    load_ids.start()
+    load_gates.start()
+    for f in range(F):
+        load(f).start()
+    for kind in range(3):
+        load_own(kind).start()
+
+    barrier = pltpu.get_barrier_semaphore()
+    for i in range(1, Z):
+        pl.semaphore_signal(barrier, inc=1, device_id={"ep": lax.rem(z + i, Z) * X + x}, device_id_type=MESH)
+    for i in range(1, X):
+        pl.semaphore_signal(barrier, inc=1, device_id={"ep": z * X + lax.rem(x + i, X)}, device_id_type=MESH)
+    for i in range(1, G):
+        pl.semaphore_signal(barrier, inc=1, device_id={"grp": lax.rem(g + i, G)}, device_id_type=MESH)
+    pl.semaphore_signal(barrier, inc=1, device_id={"tp": other}, device_id_type=MESH)
+    load_ids.wait()
+    load_gates.wait()
+    meta[z] = jnp.concatenate(
+        [ids[...].astype(jnp.float32), gates[...], jnp.zeros((4, T), jnp.float32)], axis=0
+    )
+    gains[0] = gain_out_ref[...]
+    arrived(tok.at[z], load_sem)
+    load_own(0).wait()
+    pl.semaphore_wait(barrier, Z + X + G - 2)
+
+    def along(b, f, way):
+        step = s if way == IN else -s
+        return send(
+            tok.at[b, f], tok.at[b, f], tok_send, tok_recv.at[b, f], ep=(z + step) * X + x
+        )
+
+    def onward(b, f, way):
+        step = s if way == IN else -s
+        to = jnp.where((step < 0) & (z + step == b), Z, b)
+        return send(
+            acc.at[b, f], acc.at[to, f], acc_send, acc_recv.at[to, f], ep=(z + step) * X + x
+        )
+
+    def to_line(i):
+        return send(
+            meta.at[z], meta.at[z], meta_send.at[i], meta_recv.at[z], ep=lax.rem(z + i, Z) * X + x
+        )
+
+    def to_plane(i, kind, j):
+        q = g * WG + j
+        piece = wbuf.at[x, c, kind, q]
+        return send(
+            piece, piece, wx_send.at[i], plane_sem.at[x, kind, j], ep=z * X + lax.rem(x + i, X)
+        )
+
+    def to_group(p, i, kind, j):
+        piece = wbuf.at[p, c, kind, g * WG + j]
+        return send(
+            piece, piece, wy_send.at[p, i], group_sem.at[p, g, kind, j], grp=lax.rem(g + i, G)
+        )
+
+    def native_to_core(kind):
+        block = wbuf.at[x, c, kind]
+        return send(block, block, wt_send.at[x], nat_sem.at[kind], tp=other)
+
+    def to_core(p, kind, q):
+        piece = wbuf.at[p, c, kind, q]
+        rsem = down_sem.at[p, q // SUB] if kind == 2 else wide_sem.at[p, kind]
+        return send(piece, piece, wt_send.at[p], rsem, tp=other)
+
+    for i in range(1, Z):
+        to_line(i).start()
+    for f in range(F):
+        pl.when(is_inner)(lambda f=f: along(z, f, OUT).start())
+        if f < LEAD:
+            along(z, f, IN).start()
+        else:
+            pl.when(is_end)(lambda f=f: along(z, f, IN).start())
+    for kind in range(3):
+        if kind > 0:
+            load_own(kind).wait()
+        for j in range(WG):
+            for i in range(1, X):
+                to_plane(i, kind, j).start()
+        native_to_core(kind).start()
+    gain_copy = send(gain_out_ref, gains.at[1], gain_send, gain_recv, tp=other)
+    gain_copy.start()
+
+    PIECES = 3 * WG
+
+    def tick(n):
+        if n < PIECES:
+            kind, j = n // WG, n % WG
+            q = g * WG + j
+            for i in range(1, X):
+                p = lax.rem(x + i, X)
+                arrived(wbuf.at[p, c, kind, q], plane_sem.at[p, kind, j])
+                for i2 in range(1, G):
+                    to_group(p, i2, kind, j).start()
+                to_core(p, kind, q).start()
+        if LAG <= n < PIECES + LAG:
+            kind, j = (n - LAG) // WG, (n - LAG) % WG
+            for i in range(1, X):
+                p = lax.rem(x + i, X)
+                for i2 in range(1, G):
+                    g2 = lax.rem(g + i2, G)
+                    q = g2 * WG + j
+                    arrived(wbuf.at[p, c, kind, q], group_sem.at[p, g2, kind, j])
+                    to_core(p, kind, q).start()
+
+    def native_slices(kind):
+        arrived(wbuf.at[x, other, kind], nat_sem.at[kind])
+
+    def core_slices(kind):
+        for i in range(1, X):
+            p = lax.rem(x + i, X)
+            arrived(wbuf.at[p, other, kind], wide_sem.at[p, kind])
+
+    def down_slices(f):
+        for i in range(1, X):
+            p = lax.rem(x + i, X)
+            arrived(wbuf.at[p, other, 2, pl.ds(f * SUB, SUB)], down_sem.at[p, f])
+
+    def lines():
+        for i in range(1, Z):
+            b = lax.rem(z + i, Z)
+            arrived(meta.at[b], meta_recv.at[b])
+
+    def route(b):
+        m = meta[b]
+        expert = (lax.broadcasted_iota(jnp.int32, (8, T), 0) + z * X).astype(jnp.float32)
+        first, second = m[0:1] == expert, m[1:2] == expert
+        named = jnp.where(first | second, 1.0, 0.0)
+        gate_row = jnp.where(first, m[2:3], 0.0) + jnp.where(second, m[3:4], 0.0)
+        line = lax.broadcasted_iota(jnp.int32, (T, T), 0)
+        earlier = jnp.where(line < lax.broadcasted_iota(jnp.int32, (T, T), 1), 1.0, 0.0)
+        before = jnp.dot(
+            named.astype(jnp.bfloat16), earlier.astype(jnp.bfloat16), preferred_element_type=jnp.float32
+        )
+        place = jnp.where(named > 0.0, before, -1.0)
+        slot = lax.broadcasted_iota(jnp.int32, (cap, T), 0).astype(jnp.float32)
+        for p in range(X):
+            hit = place[p : p + 1] == slot
+            pick[b, p * cap : (p + 1) * cap] = jnp.where(hit, 1.0, 0.0).astype(jnp.bfloat16)
+            weight = jnp.sum(jnp.where(hit, gate_row[p : p + 1], 0.0), axis=1, keepdims=True)
+            gslot[b, p * cap : (p + 1) * cap] = jnp.broadcast_to(weight, (cap, 128))
+
+    def gather(b):
+        square = jnp.zeros((R, 1), jnp.float32)
+        for f in range(F):
+            row = jnp.dot(pick[b], tok[b, f], preferred_element_type=jnp.float32)
+            square = square + jnp.sum(row * row, axis=1, keepdims=True)
+            rows[:, f * C : (f + 1) * C] = row.astype(jnp.bfloat16)
+        inv = lax.rsqrt(square / D + EPS)
+        for f in range(F):
+            span = slice(f * C, (f + 1) * C)
+            rows[:, span] = (rows[:, span].astype(jnp.float32) * inv * gain_in_ref[:, span]).astype(jnp.bfloat16)
+
+    def gate(b):
+        for p in range(X):
+            for half in range(2):
+                gated[p * cap : (p + 1) * cap, half * H : (half + 1) * H] = jnp.dot(
+                    rows[p * cap : (p + 1) * cap], wbuf[p, half, 0].reshape(D, H),
+                    preferred_element_type=jnp.float32,
+                )
+
+    def up(b, p):
+        span = pl.ds(pl.multiple_of(p * cap, cap), cap)
+        for half in range(2):
+            side = slice(half * H, (half + 1) * H)
+            wide = jnp.dot(rows[span], wbuf[p, half, 1].reshape(D, H), preferred_element_type=jnp.float32)
+            value = gated[span, side]
+            hid[b, span, side] = (value / (1.0 + jnp.exp(-value)) * wide).astype(jnp.bfloat16)
+
+    def hidden(b):
+        route(b)
+        gather(b)
+        gate(b)
+        for p in range(X):
+            up(b, p)
+
+    def partial(b, f):
+        parts = []
+        for p in range(X):
+            span = slice(p * cap, (p + 1) * cap)
+            low = wbuf[p, 0, 2, pl.ds(f * SUB, SUB)].reshape(C, H)
+            high = wbuf[p, 1, 2, pl.ds(f * SUB, SUB)].reshape(C, H)
+            y = lax.dot_general(
+                hid[b, span, 0:H], low, NT, preferred_element_type=jnp.float32
+            ) + lax.dot_general(
+                hid[b, span, H : 2 * H], high, NT, preferred_element_type=jnp.float32
+            )
+            parts.append((y * gslot[b, span, 0:1]).astype(jnp.bfloat16))
+        return lax.dot_general(
+            pick[b], jnp.concatenate(parts, axis=0), TN, preferred_element_type=jnp.float32
+        )
+
+    def own_part():
+        def one(f, carry):
+            comb[f] = partial(z, f)
+            return carry
+
+        lax.fori_loop(0, F, one, 0)
+
+    def begin(b, f):
+        acc[b, f] = partial(b, f).astype(jnp.bfloat16)
+        onward(b, f, IN).start()
+
+    def chain(b, f, way):
+        part = partial(b, f)
+        arrived(acc.at[b, f], acc_recv.at[b, f])
+        acc[b, f] = (part + acc[b, f].astype(jnp.float32)).astype(jnp.bfloat16)
+        onward(b, f, way).start()
+
+    near, mid, far = z + s, z + 2 * s, z + 3 * s
+    back = z - s
+
+    @pl.when(is_end)
+    def _():
+        for n in range(2 * WG):
+            tick(n)
+            if n == WG // 2:
+                lines()
+                route(near)
+        for f in range(F):
+            arrived(tok.at[near, f], tok_recv.at[near, f])
+        gather(near)
+        tick(2 * WG)
+        native_slices(0)
+        core_slices(0)
+        gate(near)
+        tick(2 * WG + 1)
+        native_slices(1)
+        up(near, x)
+        tick(2 * WG + 2)
+        core_slices(1)
+        for i in range(1, X):
+            up(near, lax.rem(x + i, X))
+        native_slices(2)
+        for j in range(FG):
+            if j < FG - 1:
+                down_slices(g * FG + j)
+                begin(near, g * FG + j)
+            for k in range(SUB):
+                tick(2 * WG + LAG + j * SUB + k)
+            if j < FG - 1:
+                for i in range(1, G):
+                    f = lax.rem(g + i, G) * FG + j
+                    down_slices(f)
+                    begin(near, f)
+        for i in range(G):
+            down_slices(i * FG + FG - 1)
+        for i in range(G - 1):
+            begin(near, i * FG + FG - 1)
+
+        def later(i, carry):
+            b = jnp.where(i == 0, far, jnp.where(i == 1, z, mid))
+
+            @pl.when(i != 1)
+            def _():
+                for f in range(F):
+                    arrived(tok.at[b, f], tok_recv.at[b, f])
+
+            hidden(b)
+
+            @pl.when(i != 1)
+            def _():
+                def one(f, inner):
+                    begin(b, f)
+                    return inner
+
+                lax.fori_loop(0, F, one, 0)
+
+            pl.when(i == 1)(own_part)
+            return carry
+
+        lax.fori_loop(0, 3, later, 0)
+        begin(near, F - 1)
+
+    @pl.when(is_inner)
+    def _():
+        def relay(b, f, way):
+            arrived(tok.at[b, f], tok_recv.at[b, f])
+            along(b, f, way).start()
+
+        for n in range(PIECES + LAG):
+            tick(n)
+            k = n // SUB
+            if n % SUB == SUB - 1 and k < F:
+                relay(back, k, IN)
+                if k == F - 1:
+                    for f in range(LEAD, F):
+                        along(z, f, IN).start()
+            k = (n - WG - 1) // SUB
+            if n > WG and (n - WG - 1) % SUB == 0 and k < F:
+                relay(mid, k, OUT)
+        for f in range(F - 4):
+            relay(near, f, OUT)
+        lines()
+        for kind in range(3):
+            native_slices(kind)
+            if kind < 2:
+                core_slices(kind)
+        for f in range(F):
+            down_slices(f)
+
+        def ready(i, carry):
+            relay(near, F - 4 + i, OUT)
+            hidden(jnp.where(i == 0, back, jnp.where(i == 1, mid, jnp.where(i == 2, z, near))))
+            return carry
+
+        lax.fori_loop(0, 4, ready, 0)
+        own_part()
+
+        def cross(i, carry):
+            k, turn = i // 2, lax.rem(i, 2)
+            pl.when((turn == 0) & (k < F))(lambda: chain(mid, k, IN))
+            pl.when((turn == 1) & (k >= 2))(lambda: chain(back, k - 2, OUT))
+            return carry
+
+        lax.fori_loop(0, 2 * (F + 2), cross, 0)
+
+        def last(f, carry):
+            chain(near, f, IN)
+            return carry
+
+        lax.fori_loop(0, F, last, 0)
+
+    total = jnp.zeros((T, 1), jnp.float32)
+    for f in range(F):
+
+        @pl.when(z > 0)
+        def _():
+            arrived(acc.at[z, f], acc_recv.at[z, f])
+            comb[f] = comb[f] + acc[z, f].astype(jnp.float32)
+
+        @pl.when(z < Z - 1)
+        def _():
+            arrived(acc.at[Z, f], acc_recv.at[Z, f])
+            comb[f] = comb[f] + acc[Z, f].astype(jnp.float32)
+
+        value = comb[f]
+        total = total + jnp.sum(value * value, axis=1, keepdims=True)
+    scale = lax.rsqrt(total / D + EPS)
+    arrived(gains.at[1], gain_recv)
+    half = F // 2
+
+    def out_copy(f):
+        return send(
+            stage.at[f], out_ref.at[c, :, f * C : (f + 1) * C], out_send, out_recv, tp=other
+        )
+
+    for f in range(half):
+        stage[f] = (comb[other * half + f] * scale * gains[1, :, f * C : (f + 1) * C]).astype(jnp.bfloat16)
+        out_copy(f).start()
+    for f in range(half):
+        out_ref[c, :, f * C : (f + 1) * C] = (
+            comb[c * half + f] * scale * gains[0, :, f * C : (f + 1) * C]
+        ).astype(jnp.bfloat16)
+
+    gain_copy.wait_send()
+    for i in range(1, Z):
+        to_line(i).wait_send()
+    for i in range(1, X):
+        p = lax.rem(x + i, X)
+        arrived(wbuf.at[x, c, :, pl.ds(0, WG)], wx_send.at[i])
+        for i2 in range(1, G):
+            arrived(wbuf.at[p, c, :, pl.ds(0, WG)], wy_send.at[p, i2])
+    for p in range(X):
+        arrived(wbuf.at[p, c], wt_send.at[p])
+    pl.when(is_end)(lambda: arrived(tok.at[z], tok_send))
+    pl.when(is_inner)(lambda: arrived(acc, tok_send))
+    arrived(acc.at[pl.ds(0, 3)], acc_send)
+    arrived(stage, out_send)
+    arrived(stage, out_recv)
+
+
 def per_device(G, X, Z, tokens, gain_in, expert_ids, gate_weights, w_gate, w_up, w_down, gain_out):
     T, D = tokens.shape
     top = expert_ids.shape[1]
     cap = 2 * T * top // (X * Z)
     H = w_gate.shape[2]
-    F = 4
+    quad = Z == 4
+    F = 8 if quad else 4
     C = D // F
-    first = lax.axis_index("tp") * T
-    ids = lax.dynamic_slice_in_dim(expert_ids, first, T, 0).astype(jnp.float32)
-    gates = lax.dynamic_slice_in_dim(gate_weights, first, T, 0)
-    meta = jnp.concatenate([ids.T, gates.T, jnp.zeros((8 - 2 * top, T), jnp.float32)], axis=0)
     vmem = pl.BlockSpec(memory_space=pltpu.VMEM)
     hbm = pl.BlockSpec(memory_space=pl.ANY)
     bf16, f32 = jnp.bfloat16, jnp.float32
     dma = pltpu.SemaphoreType.DMA
     R = X * cap
-    out = pl.pallas_call(
-        functools.partial(kernel, G, X, Z, F, cap),
-        out_shape=jax.ShapeDtypeStruct((2, T, D // 2), bf16),
-        in_specs=[hbm, vmem, vmem, hbm, hbm, hbm, vmem],
-        out_specs=vmem,
-        scratch_shapes=[
+    if quad:
+        W = 2 * F
+        body, pieces = quad_kernel, (W, D // W, H)
+        routing, specs = (expert_ids.T, gate_weights.T), [hbm, hbm]
+        scratch = [
+            pltpu.VMEM((X, 2, 3, W, D // W, H), bf16),
+            pltpu.VMEM((Z, F, T, C), bf16),
+            pltpu.VMEM((Z, 8, T), f32),
+            pltpu.VMEM((Z + 1, F, T, C), bf16),
+            pltpu.VMEM((F, T, C), f32),
+            pltpu.VMEM((R, D), bf16),
+            pltpu.VMEM((R, 2 * H), f32),
+            pltpu.VMEM((Z, R, 2 * H), bf16),
+            pltpu.VMEM((Z, R, T), bf16),
+            pltpu.VMEM((Z, R, 128), f32),
+            pltpu.VMEM((2, 1, D // 2), f32),
+            pltpu.VMEM((F // 2, T, C), bf16),
+            pltpu.VMEM((top, T), jnp.int32),
+            pltpu.VMEM((top, T), f32),
+            dma((3,)),
+            dma((3,)),
+            dma((X, 3, W // G)),
+            dma((X, G, 3, W // G)),
+            dma((X, 2)),
+            dma((X, F)),
+            dma((X,)),
+            dma((X, G)),
+            dma((X,)),
+            dma((Z, F)),
+            dma,
+            dma((Z,)),
+            dma((Z,)),
+            dma((Z + 1, F)),
+            dma,
+            dma,
+            dma,
+            dma,
+            dma,
+            dma,
+            dma((2,)),
+        ]
+    else:
+        first = lax.axis_index("tp") * T
+        ids = lax.dynamic_slice_in_dim(expert_ids, first, T, 0).astype(f32)
+        gates = lax.dynamic_slice_in_dim(gate_weights, first, T, 0)
+        meta = jnp.concatenate([ids.T, gates.T, jnp.zeros((8 - 2 * top, T), f32)], axis=0)
+        body, pieces = kernel, (F, C, H)
+        routing, specs = (meta,), [vmem]
+        scratch = [
             pltpu.VMEM((X, 2, 3, F, C, H), bf16),
             pltpu.VMEM((Z, F, T, C), bf16),
             pltpu.VMEM((Z, 8, T), f32),
@@ -401,13 +857,19 @@
             dma((2,)),
             dma((2,)),
             dma((F,)),
-        ],
+        ]
+    out = pl.pallas_call(
+        functools.partial(body, G, X, Z, F, cap),
+        out_shape=jax.ShapeDtypeStruct((2, T, D // 2), bf16),
+        in_specs=[hbm, vmem] + specs + [hbm, hbm, hbm, vmem],
+        out_specs=vmem,
+        scratch_shapes=scratch,
         compiler_params=pltpu.CompilerParams(
             collective_id=0, has_side_effects=True, vmem_limit_bytes=67043328
         ),
     )(
-        tokens, gain_in.reshape(1, D), meta,
-        w_gate.reshape(F, C, H), w_up.reshape(F, C, H), w_down.reshape(F, C, H),
+        tokens, gain_in.reshape(1, D), *routing,
+        w_gate.reshape(pieces), w_up.reshape(pieces), w_down.reshape(pieces),
         gain_out.reshape(1, D // 2),
     )
     return out.reshape(2 * T, D // 2)

time: 128 us -> 117 us (0.914)
  Pallas kernels: 123 us -> 113 us
    pallas_call x1, Pallas kernels: 123 us -> 113 us  [per_device(): pl.pallas_call(functools.partial(body, G, X, Z, F, cap), out_shape=jax.Sh...]
    unnamed x5 -> x1, local copies, waits for them, and re-layouts: 2.88 us -> 2.26 us
where the time goes in v1:
time: 117 us; the launch traced here: 115 us
  Pallas kernels  113 us (97%)
  local copies, waits for them, and re-layouts  2.26 us (2%)
    pallas_call x1, Pallas kernels, per_device(): pl.pallas_call(functools.partial(body, G, X, Z, F, cap), out_shape=jax.Sh...  113 us

profile of v1, /device:TPU:11, one launch (start us, length us, event | category | flops | bytes accessed | tf_op | source)
XLA Modules:
  0.0 115.2 jit_solution(7040125070827108892)
XLA Ops:
  0.0 112.9 %shard_map.82 = bf16[2,256,1024]{2,1,0:T(8,128)(2,1)} custom-call(bf16[256,2048]{1,0:T(8,128)(2,1)} %tokens_ref.1, f32[1,2048]{1,0:T(1,128)} %bitcast.12, s32[2,512]{1,0:T(2,128)} %bitcast.13, f32[2,512]{1,0:T(2,128)} %bitcast.14, bf16[16,128,256]{2,1,0:T(8,128)(2,1)} %bitcast.9, bf16[16,128,256]{2,1,0:T(8,128)(2,1)} %bitcast.10, ...), custom_call_target="tpu_custom_call" | custom-call | tf_op jit(solution)/shard_map/pallas_call | solution.py:861
  112.9 2.3 %copy.10 = bf16[512,1024]{1,0:T(8,128)(2,1)} copy(bf16[512,1024]{1,0:T(8,128)(2,1)} %bitcast.8) | data formatting | bytes 2097152

commit v2 on v1

--- a/solution.py
+++ b/solution.py
@@ -359,7 +359,7 @@
     G, X, Z, F, cap,
     tokens_ref, gain_in_ref, ids_ref, gates_ref, wg_ref, wu_ref, wd_ref, gain_out_ref,
     out_ref,
-    wbuf, tok, meta, acc, comb, rows, gated, hid, pick, gslot, gains, stage, ids, gates,
+    wbuf, tok, meta, acc, comb, rows, gated, hid, pick, gslot, gains, stage, ids, gates, gain_row,
     own_sem, nat_sem, plane_sem, group_sem, wide_sem, down_sem, wx_send, wy_send, wt_send,
     tok_recv, tok_send, meta_recv, meta_send, acc_recv, acc_send,
     gain_recv, gain_send, out_recv, out_send, load_sem, pair_sem,
@@ -391,20 +391,23 @@
         )
 
     def load(f):
-        return pltpu.make_async_copy(tokens_ref.at[:, f * C : (f + 1) * C], tok.at[z, f], load_sem)
+        return pltpu.make_async_copy(
+            tokens_ref.at[:, f * C : (f + 1) * C], tok.at[z, f], load_sem.at[f // LEAD]
+        )
 
     def load_own(kind):
         return pltpu.make_async_copy(weights[kind], wbuf.at[x, c, kind], own_sem.at[kind])
 
     mine = pl.ds(pl.multiple_of(c * T, T), T)
-    load_ids = pltpu.make_async_copy(ids_ref.at[:, mine], ids, pair_sem.at[0])
-    load_gates = pltpu.make_async_copy(gates_ref.at[:, mine], gates, pair_sem.at[1])
-    load_ids.start()
-    load_gates.start()
-    for f in range(F):
+    small = (
+        pltpu.make_async_copy(ids_ref.at[:, mine], ids, pair_sem.at[0]),
+        pltpu.make_async_copy(gates_ref.at[:, mine], gates, pair_sem.at[1]),
+        pltpu.make_async_copy(gain_out_ref, gains.at[0], pair_sem.at[2]),
+        pltpu.make_async_copy(gain_in_ref, gain_row, pair_sem.at[3]),
+    )
+    for f in range(LEAD):
         load(f).start()
-    for kind in range(3):
-        load_own(kind).start()
+    load_own(0).start()
 
     barrier = pltpu.get_barrier_semaphore()
     for i in range(1, Z):
@@ -414,21 +417,21 @@
     for i in range(1, G):
         pl.semaphore_signal(barrier, inc=1, device_id={"grp": lax.rem(g + i, G)}, device_id_type=MESH)
     pl.semaphore_signal(barrier, inc=1, device_id={"tp": other}, device_id_type=MESH)
-    load_ids.wait()
-    load_gates.wait()
-    meta[z] = jnp.concatenate(
-        [ids[...].astype(jnp.float32), gates[...], jnp.zeros((4, T), jnp.float32)], axis=0
-    )
-    gains[0] = gain_out_ref[...]
-    arrived(tok.at[z], load_sem)
-    load_own(0).wait()
+    for piece in small:
+        piece.start()
+    for f in range(LEAD, F):
+        load(f).start()
     pl.semaphore_wait(barrier, Z + X + G - 2)
 
     def along(b, f, way):
         step = s if way == IN else -s
         return send(
-            tok.at[b, f], tok.at[b, f], tok_send, tok_recv.at[b, f], ep=(z + step) * X + x
-        )
+            tok.at[b, f], tok.at[b, f], tok_send, tok_recv.at[lax.rem(b - z - step + Z, Z) - 1, f],
+            ep=(z + step) * X + x,
+        )
+
+    def token(b, f):
+        arrived(tok.at[b, f], tok_recv.at[lax.rem(b - z + Z, Z) - 1, f])
 
     def onward(b, f, way):
         step = s if way == IN else -s
@@ -446,13 +449,18 @@
         q = g * WG + j
         piece = wbuf.at[x, c, kind, q]
         return send(
-            piece, piece, wx_send.at[i], plane_sem.at[x, kind, j], ep=z * X + lax.rem(x + i, X)
-        )
+            piece, piece, wx_send.at[i], plane_sem.at[X - i - 1, kind, j],
+            ep=z * X + lax.rem(x + i, X),
+        )
+
+    def ahead(p):
+        return lax.rem(p - x + X, X) - 1
 
     def to_group(p, i, kind, j):
         piece = wbuf.at[p, c, kind, g * WG + j]
         return send(
-            piece, piece, wy_send.at[p, i], group_sem.at[p, g, kind, j], grp=lax.rem(g + i, G)
+            piece, piece, wy_send.at[p, i], group_sem.at[ahead(p), G - i - 1, kind, j],
+            grp=lax.rem(g + i, G),
         )
 
     def native_to_core(kind):
@@ -461,26 +469,41 @@
 
     def to_core(p, kind, q):
         piece = wbuf.at[p, c, kind, q]
-        rsem = down_sem.at[p, q // SUB] if kind == 2 else wide_sem.at[p, kind]
+        rsem = down_sem.at[ahead(p), q // SUB] if kind == 2 else wide_sem.at[ahead(p), kind]
         return send(piece, piece, wt_send.at[p], rsem, tp=other)
 
-    for i in range(1, Z):
-        to_line(i).start()
-    for f in range(F):
-        pl.when(is_inner)(lambda f=f: along(z, f, OUT).start())
-        if f < LEAD:
-            along(z, f, IN).start()
-        else:
-            pl.when(is_end)(lambda f=f: along(z, f, IN).start())
-    for kind in range(3):
-        if kind > 0:
-            load_own(kind).wait()
+    def own_tokens(low, high):
+        arrived(tok.at[z, pl.ds(low, high - low)], load_sem.at[low // LEAD])
+        for f in range(low, high):
+            pl.when(is_inner)(lambda f=f: along(z, f, OUT).start())
+            if f < LEAD:
+                along(z, f, IN).start()
+            else:
+                pl.when(is_end)(lambda f=f: along(z, f, IN).start())
+
+    def own_weights(kind):
+        load_own(kind).wait()
         for j in range(WG):
             for i in range(1, X):
                 to_plane(i, kind, j).start()
         native_to_core(kind).start()
-    gain_copy = send(gain_out_ref, gains.at[1], gain_send, gain_recv, tp=other)
+
+    own_tokens(0, LEAD)
+    own_weights(0)
+    load_own(1).start()
+    load_own(2).start()
+    for piece in small:
+        piece.wait()
+    meta[z] = jnp.concatenate(
+        [ids[...].astype(jnp.float32), gates[...], jnp.zeros((8 - 2 * ids.shape[0], T), jnp.float32)], axis=0
+    )
+    gain_copy = send(gains.at[0], gains.at[1], gain_send, gain_recv, tp=other)
     gain_copy.start()
+    for i in range(1, Z):
+        to_line(i).start()
+    own_tokens(LEAD, F)
+    own_weights(1)
+    own_weights(2)
 
     PIECES = 3 * WG
 
@@ -490,7 +513,7 @@
             q = g * WG + j
             for i in range(1, X):
                 p = lax.rem(x + i, X)
-                arrived(wbuf.at[p, c, kind, q], plane_sem.at[p, kind, j])
+                arrived(wbuf.at[p, c, kind, q], plane_sem.at[i - 1, kind, j])
                 for i2 in range(1, G):
                     to_group(p, i2, kind, j).start()
                 to_core(p, kind, q).start()
@@ -501,7 +524,7 @@
                 for i2 in range(1, G):
                     g2 = lax.rem(g + i2, G)
                     q = g2 * WG + j
-                    arrived(wbuf.at[p, c, kind, q], group_sem.at[p, g2, kind, j])
+                    arrived(wbuf.at[p, c, kind, q], group_sem.at[i - 1, i2 - 1, kind, j])
                     to_core(p, kind, q).start()
 
     def native_slices(kind):
@@ -510,12 +533,12 @@
     def core_slices(kind):
         for i in range(1, X):
             p = lax.rem(x + i, X)
-            arrived(wbuf.at[p, other, kind], wide_sem.at[p, kind])
+            arrived(wbuf.at[p, other, kind], wide_sem.at[i - 1, kind])
 
     def down_slices(f):
         for i in range(1, X):
             p = lax.rem(x + i, X)
-            arrived(wbuf.at[p, other, 2, pl.ds(f * SUB, SUB)], down_sem.at[p, f])
+            arrived(wbuf.at[p, other, 2, pl.ds(f * SUB, SUB)], down_sem.at[i - 1, f])
 
     def lines():
         for i in range(1, Z):
@@ -550,7 +573,7 @@
         inv = lax.rsqrt(square / D + EPS)
         for f in range(F):
             span = slice(f * C, (f + 1) * C)
-            rows[:, span] = (rows[:, span].astype(jnp.float32) * inv * gain_in_ref[:, span]).astype(jnp.bfloat16)
+            rows[:, span] = (rows[:, span].astype(jnp.float32) * inv * gain_row[:, span]).astype(jnp.bfloat16)
 
     def gate(b):
         for p in range(X):
@@ -619,7 +642,7 @@
                 lines()
                 route(near)
         for f in range(F):
-            arrived(tok.at[near, f], tok_recv.at[near, f])
+            token(near, f)
         gather(near)
         tick(2 * WG)
         native_slices(0)
@@ -655,7 +678,7 @@
             @pl.when(i != 1)
             def _():
                 for f in range(F):
-                    arrived(tok.at[b, f], tok_recv.at[b, f])
+                    token(b, f)
 
             hidden(b)
 
@@ -676,7 +699,7 @@
     @pl.when(is_inner)
     def _():
         def relay(b, f, way):
-            arrived(tok.at[b, f], tok_recv.at[b, f])
+            token(b, f)
             along(b, f, way).start()
 
         for n in range(PIECES + LAG):
@@ -710,17 +733,11 @@
 
         def cross(i, carry):
             k, turn = i // 2, lax.rem(i, 2)
-            pl.when((turn == 0) & (k < F))(lambda: chain(mid, k, IN))
-            pl.when((turn == 1) & (k >= 2))(lambda: chain(back, k - 2, OUT))
+            pl.when(turn == 0)(lambda: chain(jnp.where(k < F, mid, near), lax.rem(k, F), IN))
+            pl.when((turn == 1) & (k >= 2) & (k < F + 2))(lambda: chain(back, k - 2, OUT))
             return carry
 
-        lax.fori_loop(0, 2 * (F + 2), cross, 0)
-
-        def last(f, carry):
-            chain(near, f, IN)
-            return carry
-
-        lax.fori_loop(0, F, last, 0)
+        lax.fori_loop(0, 4 * F, cross, 0)
 
     total = jnp.zeros((T, 1), jnp.float32)
     for f in range(F):
@@ -787,7 +804,7 @@
     if quad:
         W = 2 * F
         body, pieces = quad_kernel, (W, D // W, H)
-        routing, specs = (expert_ids.T, gate_weights.T), [hbm, hbm]
+        routing, specs = (expert_ids.T, gate_weights.T), [hbm] * 8
         scratch = [
             pltpu.VMEM((X, 2, 3, W, D // W, H), bf16),
             pltpu.VMEM((Z, F, T, C), bf16),
@@ -803,16 +820,17 @@
             pltpu.VMEM((F // 2, T, C), bf16),
             pltpu.VMEM((top, T), jnp.int32),
             pltpu.VMEM((top, T), f32),
+            pltpu.VMEM((1, D), f32),
             dma((3,)),
             dma((3,)),
-            dma((X, 3, W // G)),
-            dma((X, G, 3, W // G)),
-            dma((X, 2)),
-            dma((X, F)),
+            dma((X - 1, 3, W // G)),
+            dma((X - 1, G - 1, 3, W // G)),
+            dma((X - 1, 2)),
+            dma((X - 1, F)),
             dma((X,)),
             dma((X, G)),
             dma((X,)),
-            dma((Z, F)),
+            dma((Z - 1, F)),
             dma,
             dma((Z,)),
             dma((Z,)),
@@ -822,16 +840,20 @@
             dma,
             dma,
             dma,
-            dma,
             dma((2,)),
+            dma((4,)),
         ]
+        out_type = pltpu.VMEM((2, T, D // 2), bf16)
+        limit = 67043328 - 2 * T * D
     else:
         first = lax.axis_index("tp") * T
         ids = lax.dynamic_slice_in_dim(expert_ids, first, T, 0).astype(f32)
         gates = lax.dynamic_slice_in_dim(gate_weights, first, T, 0)
         meta = jnp.concatenate([ids.T, gates.T, jnp.zeros((8 - 2 * top, T), f32)], axis=0)
         body, pieces = kernel, (F, C, H)
-        routing, specs = (meta,), [vmem]
+        routing, specs = (meta,), [hbm, vmem, vmem, hbm, hbm, hbm, vmem]
+        out_type = jax.ShapeDtypeStruct((2, T, D // 2), bf16)
+        limit = 67043328
         scratch = [
             pltpu.VMEM((X, 2, 3, F, C, H), bf16),
             pltpu.VMEM((Z, F, T, C), bf16),
@@ -860,12 +882,12 @@
         ]
     out = pl.pallas_call(
         functools.partial(body, G, X, Z, F, cap),
-        out_shape=jax.ShapeDtypeStruct((2, T, D // 2), bf16),
-        in_specs=[hbm, vmem] + specs + [hbm, hbm, hbm, vmem],
+        out_shape=out_type,
+        in_specs=specs,
         out_specs=vmem,
         scratch_shapes=scratch,
         compiler_params=pltpu.CompilerParams(
-            collective_id=0, has_side_effects=True, vmem_limit_bytes=67043328
+            collective_id=0, has_side_effects=True, vmem_limit_bytes=limit
         ),
     )(
         tokens, gain_in.reshape(1, D), *routing,

time: 117 us -> 114 us (0.974); the launches traced: 115 us -> 114 us
  local copies, waits for them, and re-layouts: 2.26 us -> 0.97 us
    unnamed x1, local copies, waits for them, and re-layouts: 2.26 us -> 0.97 us
where the time goes in v2:
time: 114 us
  Pallas kernels  113 us (99%)
    pallas_call x1, Pallas kernels, per_device(): pl.pallas_call(functools.partial(body, G, X, Z, F, cap), out_shape=out_ty...  113 us

profile of v2, /device:TPU:11, one launch (start us, length us, event | category | flops | bytes accessed | tf_op | source)
XLA Modules:
  0.0 113.7 jit_solution(1372065623365304124)
XLA Ops:
  0.0 112.8 %shard_map.82 = bf16[2,256,1024]{2,1,0:T(8,128)(2,1)S(1)} custom-call(bf16[256,2048]{1,0:T(8,128)(2,1)} %tokens_ref.1, f32[1,2048]{1,0:T(1,128)} %bitcast.12, s32[2,512]{1,0:T(2,128)} %bitcast.13, f32[2,512]{1,0:T(2,128)} %bitcast.14, bf16[16,128,256]{2,1,0:T(8,128)(2,1)} %bitcast.9, bf16[16,128,256]{2,1,0:T(8,128)(2,1)} %bitcast.10, ...), custom_call_target="tpu_custom_call" | custom-call | tf_op jit(solution)/shard_map/pallas_call | solution.py:883
  112.8 1.0 copy.10

commit v3 on v2

--- a/solution.py
+++ b/solution.py
@@ -440,6 +440,17 @@
             acc.at[b, f], acc.at[to, f], acc_send, acc_recv.at[to, f], ep=(z + step) * X + x
         )
 
+    def halves(b, f, h):
+        return acc.at[b, f, pl.ds(h * T // 2, T // 2)]
+
+    def onward_half(b, h, way):
+        step = s if way == IN else -s
+        to = jnp.where((step < 0) & (z + step == b), Z, b)
+        return send(
+            halves(b, F - 1, h), halves(to, F - 1, h), acc_send, acc_recv.at[to, F - 1 + h],
+            ep=(z + step) * X + x,
+        )
+
     def to_line(i):
         return send(
             meta.at[z], meta.at[z], meta_send.at[i], meta_recv.at[z], ep=lax.rem(z + i, Z) * X + x
@@ -482,14 +493,14 @@
                 pl.when(is_end)(lambda f=f: along(z, f, IN).start())
 
     def own_weights(kind):
-        load_own(kind).wait()
         for j in range(WG):
             for i in range(1, X):
                 to_plane(i, kind, j).start()
-        native_to_core(kind).start()
 
     own_tokens(0, LEAD)
+    load_own(0).wait()
     own_weights(0)
+    native_to_core(0).start()
     load_own(1).start()
     load_own(2).start()
     for piece in small:
@@ -502,8 +513,12 @@
     for i in range(1, Z):
         to_line(i).start()
     own_tokens(LEAD, F)
+    load_own(1).wait()
     own_weights(1)
-    own_weights(2)
+    native_to_core(1).start()
+    load_own(2).wait()
+    pl.when(c == 0)(lambda: own_weights(2))
+    native_to_core(2).start()
 
     PIECES = 3 * WG
 
@@ -623,13 +638,29 @@
 
     def begin(b, f):
         acc[b, f] = partial(b, f).astype(jnp.bfloat16)
-        onward(b, f, IN).start()
+        pl.when(f != F - 1)(lambda: onward(b, f, IN).start())
+
+        @pl.when(f == F - 1)
+        def _():
+            for h in range(2):
+                onward_half(b, h, IN).start()
 
     def chain(b, f, way):
         part = partial(b, f)
-        arrived(acc.at[b, f], acc_recv.at[b, f])
-        acc[b, f] = (part + acc[b, f].astype(jnp.float32)).astype(jnp.bfloat16)
-        onward(b, f, way).start()
+
+        @pl.when(f != F - 1)
+        def _():
+            arrived(acc.at[b, f], acc_recv.at[b, f])
+            acc[b, f] = (part + acc[b, f].astype(jnp.float32)).astype(jnp.bfloat16)
+            onward(b, f, way).start()
+
+        @pl.when(f == F - 1)
+        def _():
+            for h in range(2):
+                span = slice(h * T // 2, (h + 1) * T // 2)
+                arrived(halves(b, F - 1, h), acc_recv.at[b, F - 1 + h])
+                acc[b, F - 1, span] = (part[span] + acc[b, F - 1, span].astype(jnp.float32)).astype(jnp.bfloat16)
+                onward_half(b, h, way).start()
 
     near, mid, far = z + s, z + 2 * s, z + 3 * s
     back = z - s
@@ -641,6 +672,7 @@
             if n == WG // 2:
                 lines()
                 route(near)
+        pl.when(c != 0)(lambda: own_weights(2))
         for f in range(F):
             token(near, f)
         gather(near)
@@ -669,8 +701,6 @@
                     begin(near, f)
         for i in range(G):
             down_slices(i * FG + FG - 1)
-        for i in range(G - 1):
-            begin(near, i * FG + FG - 1)
 
         def later(i, carry):
             b = jnp.where(i == 0, far, jnp.where(i == 1, z, mid))
@@ -694,7 +724,8 @@
             return carry
 
         lax.fori_loop(0, 3, later, 0)
-        begin(near, F - 1)
+        for i in range(G):
+            begin(near, i * FG + FG - 1)
 
     @pl.when(is_inner)
     def _():
@@ -704,6 +735,8 @@
 
         for n in range(PIECES + LAG):
             tick(n)
+            if n == 2 * WG - 1:
+                pl.when(c != 0)(lambda: own_weights(2))
             k = n // SUB
             if n % SUB == SUB - 1 and k < F:
                 relay(back, k, IN)
@@ -740,18 +773,18 @@
         lax.fori_loop(0, 4 * F, cross, 0)
 
     total = jnp.zeros((T, 1), jnp.float32)
-    for f in range(F):
-
-        @pl.when(z > 0)
-        def _():
-            arrived(acc.at[z, f], acc_recv.at[z, f])
-            comb[f] = comb[f] + acc[z, f].astype(jnp.float32)
-
-        @pl.when(z < Z - 1)
-        def _():
-            arrived(acc.at[Z, f], acc_recv.at[Z, f])
-            comb[f] = comb[f] + acc[Z, f].astype(jnp.float32)
-
+    for f in sorted(range(F), key=lambda f: f % FG == FG - 1):
+
+        def join(slot):
+            if f < F - 1:
+                arrived(acc.at[slot, f], acc_recv.at[slot, f])
+            else:
+                for h in range(2):
+                    arrived(halves(slot, f, h), acc_recv.at[slot, f + h])
+            comb[f] = comb[f] + acc[slot, f].astype(jnp.float32)
+
+        pl.when(z > 0)(lambda: join(z))
+        pl.when(z < Z - 1)(lambda: join(Z))
         value = comb[f]
         total = total + jnp.sum(value * value, axis=1, keepdims=True)
     scale = lax.rsqrt(total / D + EPS)
@@ -834,7 +867,7 @@
             dma,
             dma((Z,)),
             dma((Z,)),
-            dma((Z + 1, F)),
+            dma((Z + 1, F + 1)),
             dma,
             dma,
             dma,

time: 114 us -> 111 us (0.974)
  Pallas kernels: 113 us -> 110 us
    pallas_call x1, Pallas kernels: 113 us -> 110 us  [per_device(): pl.pallas_call(functools.partial(body, G, X, Z, F, cap), out_shape=out_ty...]
where the time goes in v3:
time: 111 us
  Pallas kernels  110 us (99%)
    pallas_call x1, Pallas kernels, per_device(): pl.pallas_call(functools.partial(body, G, X, Z, F, cap), out_shape=out_ty...  110 us

profile of v3, /device:TPU:11, one launch (start us, length us, event | category | flops | bytes accessed | tf_op | source)
XLA Modules:
  0.0 110.7 jit_solution(3356748827692314529)
XLA Ops:
  0.0 109.8 %shard_map.82 = bf16[2,256,1024]{2,1,0:T(8,128)(2,1)S(1)} custom-call(bf16[256,2048]{1,0:T(8,128)(2,1)} %tokens_ref.1, f32[1,2048]{1,0:T(1,128)} %bitcast.12, s32[2,512]{1,0:T(2,128)} %bitcast.13, f32[2,512]{1,0:T(2,128)} %bitcast.14, bf16[16,128,256]{2,1,0:T(8,128)(2,1)} %bitcast.9, bf16[16,128,256]{2,1,0:T(8,128)(2,1)} %bitcast.10, ...), custom_call_target="tpu_custom_call" | custom-call | tf_op jit(solution)/shard_map/pallas_call | solution.py:916
  109.8 1.0 copy.10

commit v4 on v3

--- a/solution.py
+++ b/solution.py
@@ -688,19 +688,22 @@
         for i in range(1, X):
             up(near, lax.rem(x + i, X))
         native_slices(2)
-        for j in range(FG):
+        def early(j, i):
+            f = lax.rem(g + i, G) * FG + j
+            down_slices(f)
             if j < FG - 1:
-                down_slices(g * FG + j)
-                begin(near, g * FG + j)
-            for k in range(SUB):
-                tick(2 * WG + LAG + j * SUB + k)
-            if j < FG - 1:
-                for i in range(1, G):
-                    f = lax.rem(g + i, G) * FG + j
-                    down_slices(f)
-                    begin(near, f)
-        for i in range(G):
-            down_slices(i * FG + FG - 1)
+                begin(near, f)
+
+        early(0, 0)
+        for n in range(2 * WG + LAG, PIECES + LAG):
+            tick(n)
+            for j in range(FG):
+                full = 2 * WG + SUB * (j + 1) - 1
+                if n == full and j > 0:
+                    early(j, 0)
+                if n == full + LAG:
+                    for i in range(1, G):
+                        early(j, i)
 
         def later(i, carry):
             b = jnp.where(i == 0, far, jnp.where(i == 1, z, mid))

time: 111 us -> 111 us (level)
  no operation moved by 1% of the time
where the time goes in v4:
time: 111 us
  Pallas kernels  110 us (99%)
    pallas_call x1, Pallas kernels, per_device(): pl.pallas_call(functools.partial(body, G, X, Z, F, cap), out_shape=out_ty...  110 us

profile of v4, /device:TPU:11, one launch (start us, length us, event | category | flops | bytes accessed | tf_op | source)
XLA Modules:
  0.0 111.0 jit_solution(239254308790829499)
XLA Ops:
  0.0 110.0 %shard_map.82 = bf16[2,256,1024]{2,1,0:T(8,128)(2,1)S(1)} custom-call(bf16[256,2048]{1,0:T(8,128)(2,1)} %tokens_ref.1, f32[1,2048]{1,0:T(1,128)} %bitcast.12, s32[2,512]{1,0:T(2,128)} %bitcast.13, f32[2,512]{1,0:T(2,128)} %bitcast.14, bf16[16,128,256]{2,1,0:T(8,128)(2,1)} %bitcast.9, bf16[16,128,256]{2,1,0:T(8,128)(2,1)} %bitcast.10, ...), custom_call_target="tpu_custom_call" | custom-call | tf_op jit(solution)/shard_map/pallas_call | solution.py:919
  110.0 1.0 copy.10
